TPU v7x, 32 devices: a whole 2x2x4 slice. The times are simulated.
32 devices in a mesh: sp: 8 (over z, y), tp: 4 (over x, core).
Axes of the slice: x: 2, y: 2, z: 4, core: 2. Of those that a mesh axis runs over, the one named last changes fastest.
Arguments:
- resid_stream: bfloat16 [3072, 2048], P('sp'), may hold values from -6 to 6
- q_latent: bfloat16 [3072, 512], P('sp'), may hold values from -6 to 6
- kv_latent: bfloat16 [3072, 256], P('sp'), may hold values from -6 to 6
- rope_key: bfloat16 [3072, 64], P('sp'), may hold values from -6 to 6
- doc_ids: int32 [3072], P('sp'), may hold values from 0 to 3, as said below
- q_gain: float32 [512], replicated, may hold values from 1.5 to 64
- kv_gain: float32 [256], replicated, may hold values from 0.1 to 1.9
- w_query: bfloat16 [512, 3072], P(None, 'tp'), may hold values from -0.25 to 0.25
- w_key: bfloat16 [256, 2048], P(None, 'tp'), may hold values from -0.375 to 0.375
- w_value: bfloat16 [256, 2048], P(None, 'tp'), may hold values from -0.375 to 0.375
- w_out: bfloat16 [2048, 2048], replicated, may hold values from -0.5 to 0.5
- mix_gain: float32 [2048], replicated, may hold values from 0.1 to 1.9
- w_gate: bfloat16 [2048, 5632], P('sp', 'tp'), may hold values from -0.125 to 0.125
- w_up: bfloat16 [2048, 5632], P('sp', 'tp'), may hold values from -0.125 to 0.125
- w_down: bfloat16 [5632, 2048], P('tp', 'sp'), may hold values from -0.3125 to 0.3125
- out_gain: float32 [2048], replicated, may hold values from 0.1 to 1.9
Outputs:
- layer_out: bfloat16 [3072, 2048], P(('sp', 'tp'))
Inputs may be any that keep to these rules, and one draw needn't show every extreme that they name: `doc_ids`: document numbers never fall along the sequence; every document has 1 to 2304 positions and one has exactly 2304.
All inputs are finite; a program needn't handle non-finite values.
Results may differ from a plain program's by a relative error of at most 0.02.
The roundings to bfloat16 on the way count: a program that leaves them out, or rounds other values in their place, can miss the bound.
Values may be sent and summed in bfloat16 or wider, within the bound.
A program may use at most 128 MiB of HBM per device.

v0:
```python
import jax
import jax.numpy as jnp
from jax import lax
from jax.sharding import PartitionSpec as P

NOPE = 128
RD = 64
VD = 128


eps_norm = 1e-05
rope_theta = 10000.0
resid_alpha = 8.0**0.25
key_span = 2048


def rope_angles(positions):
    frequency = rope_theta ** (-jnp.arange(0, RD, 2, dtype=jnp.float32) / RD)
    angles = positions.astype(jnp.float32)[:, None] * frequency[None, :]
    return (jnp.cos(angles), jnp.sin(angles))


def rotate(values, cos_table, sin_table):
    half_width = values.shape[-1] // 2
    first_half = values[..., :half_width]
    second_half = values[..., half_width:]
    return jnp.concatenate(
        [
            first_half * cos_table - second_half * sin_table,
            second_half * cos_table + first_half * sin_table,
        ],
        axis=-1,
    )


def rms_scaled(latent, scaling):
    widened = latent.astype(jnp.float32)
    inverse = lax.rsqrt(jnp.mean(widened * widened, axis=-1, keepdims=True) + eps_norm)
    return (widened * inverse * scaling).astype(jnp.bfloat16)


def layer_scaled(stream, scaling):
    centre = stream - jnp.mean(stream, axis=-1, keepdims=True)
    spread = jnp.mean(centre * centre, axis=-1, keepdims=True)
    return centre * lax.rsqrt(spread + eps_norm) * scaling


def fold_in_blocks(carried, piece_part, attend_fn):
    piece_rows = piece_part[0].shape[0]
    if piece_rows > key_span and piece_rows % key_span == 0:

        def one_block(inner, block_index):
            sliced = tuple(
                (
                    lax.dynamic_slice_in_dim(
                        member, (block_index * key_span).astype(jnp.int32), key_span, 0
                    )
                    for member in piece_part
                )
            )
            return (attend_fn(inner, sliced), None)

        outcome = lax.scan(one_block, carried, jnp.arange(piece_rows // key_span, dtype=jnp.int32))
        return outcome[0]
    return attend_fn(carried, piece_part)


def body(
    resid_stream,
    q_latent,
    kv_latent,
    rope_key,
    doc_ids,
    q_gain,
    kv_gain,
    w_query,
    w_key,
    w_value,
    w_out,
    mix_gain,
    w_gate,
    w_up,
    w_down,
    out_gain,
):
    tok_rows = q_latent.shape[0]
    head_count = w_key.shape[1] // NOPE
    tp_count = lax.axis_size("tp")
    part_rows = tok_rows // tp_count
    tp_index = lax.axis_index("tp")
    positions = lax.axis_index("sp") * tok_rows + jnp.arange(tok_rows, dtype=jnp.int32)
    cos_table, sin_table = rope_angles(positions)
    q_normed = rms_scaled(q_latent, q_gain)
    queries = jnp.dot(q_normed, w_query, preferred_element_type=jnp.float32).reshape(
        tok_rows, head_count, NOPE + RD
    )
    query_nope = queries[:, :, :NOPE].astype(jnp.bfloat16)
    query_rope = rotate(queries[:, :, NOPE:], cos_table[:, None, :], sin_table[:, None, :]).astype(
        jnp.bfloat16
    )
    kv_normed = rms_scaled(kv_latent, kv_gain)
    key_rot = rotate(rope_key.astype(jnp.float32), cos_table, sin_table).astype(jnp.bfloat16)
    score_scale = (NOPE + RD) ** (-0.5)

    def attend_rows(carried, piece_part):
        row_top, denom_sum, accum_out = carried
        key_piece, value_piece, rot_piece, doc_piece = piece_part
        piece_rows = key_piece.shape[0]
        keys_heads = key_piece.reshape(piece_rows, head_count, NOPE)
        values_heads = value_piece.reshape(piece_rows, head_count, VD)
        scores = jnp.einsum(
            "qhd,khd->hqk", query_nope, keys_heads, preferred_element_type=jnp.float32
        )
        scores = (
            scores
            + jnp.einsum("qhd,kd->hqk", query_rope, rot_piece, preferred_element_type=jnp.float32)
        ) * score_scale
        same_doc = (doc_ids[:, None] == doc_piece[None, :])[None]
        masked = jnp.where(same_doc, scores, -1e30)
        new_top = jnp.maximum(row_top, jnp.max(masked, axis=-1))
        weights = jnp.where(same_doc, jnp.exp(masked - new_top[:, :, None]), 0.0)
        factor = jnp.exp(row_top - new_top)
        denom_sum = denom_sum * factor + jnp.sum(weights, axis=-1)
        update = jnp.einsum(
            "hqk,khd->qhd",
            weights.astype(jnp.bfloat16),
            values_heads,
            preferred_element_type=jnp.float32,
        )
        accum_out = accum_out * jnp.transpose(factor)[:, :, None] + update
        return (new_top, denom_sum, accum_out)

    initial = (
        jnp.full((head_count, tok_rows), -1e30, jnp.float32),
        jnp.zeros((head_count, tok_rows), jnp.float32),
        jnp.zeros((tok_rows, head_count, VD), jnp.float32),
    )

    def project_rows(carried, piece_part):
        latent_piece, rot_piece, doc_piece = piece_part
        key_piece = jnp.dot(latent_piece, w_key, preferred_element_type=jnp.float32).astype(
            jnp.bfloat16
        )
        value_piece = jnp.dot(latent_piece, w_value, preferred_element_type=jnp.float32).astype(
            jnp.bfloat16
        )
        return attend_rows(carried, (key_piece, value_piece, rot_piece, doc_piece))

    carried_out = fold_in_blocks(
        initial,
        (
            lax.all_gather(kv_normed, "sp", axis=0, tiled=True),
            lax.all_gather(key_rot, "sp", axis=0, tiled=True),
            lax.all_gather(doc_ids, "sp", axis=0, tiled=True),
        ),
        project_rows,
    )
    denom_sum = carried_out[1]
    attended = (
        (carried_out[2] / jnp.transpose(denom_sum)[:, :, None])
        .astype(jnp.bfloat16)
        .reshape(tok_rows, head_count * VD)
    )
    heads_rows = lax.all_to_all(attended, "tp", split_axis=0, concat_axis=1, tiled=True)
    mixer_out = jnp.dot(heads_rows, w_out, preferred_element_type=jnp.float32)
    own_resid = lax.dynamic_slice_in_dim(resid_stream, tp_index * part_rows, part_rows, 0)
    own_normed = layer_scaled(
        resid_alpha * own_resid.astype(jnp.float32) + mixer_out, mix_gain
    ).astype(jnp.bfloat16)
    normed_rows = lax.all_gather(own_normed, "tp", axis=0, tiled=True)
    gate_part = jnp.dot(
        normed_rows,
        lax.all_gather(w_gate, "sp", axis=0, tiled=True),
        preferred_element_type=jnp.float32,
    )
    up_part = jnp.dot(
        normed_rows,
        lax.all_gather(w_up, "sp", axis=0, tiled=True),
        preferred_element_type=jnp.float32,
    )
    hidden = (jax.nn.silu(gate_part) * up_part).astype(jnp.bfloat16)
    down_term = jnp.dot(
        hidden, lax.all_gather(w_down, "sp", axis=1, tiled=True), preferred_element_type=jnp.float32
    )
    ffn_sum = lax.psum_scatter(
        down_term.astype(jnp.bfloat16), "tp", scatter_dimension=0, tiled=True
    ).astype(jnp.float32)
    layer_out = layer_scaled(
        resid_alpha * own_normed.astype(jnp.float32) + 0.5 * ffn_sum, out_gain
    ).astype(jnp.bfloat16)
    return layer_out


def solution(mesh):
    in_specs = (
        P("sp", None),
        P("sp", None),
        P("sp", None),
        P("sp", None),
        P("sp"),
        P(),
        P(),
        P(None, "tp"),
        P(None, "tp"),
        P(None, "tp"),
        P(),
        P(),
        P("sp", "tp"),
        P("sp", "tp"),
        P("tp", "sp"),
        P(),
    )
    out_specs = P(("sp", "tp"), None)
    return jax.shard_map(body, mesh=mesh, in_specs=in_specs, out_specs=out_specs, check_vma=False)
```

profile of v0, /device:TPU:0, one launch (start us, length us, event | category | flops | bytes accessed | tf_op | source)
XLA Modules:
  0.0 487.2 jit_solution(11520643036253584039)
XLA Ops:
  6.5 1.1 fusion.26
  7.7 1.7 fusion.28
  9.5 0.8 convert_element_type.64
  10.3 0.7 reshape.152
  11.0 27.9 %all-gather = s32[8,1,384]{2,1,0:T(1,128)S(1)} all-gather(s32[1,1,384]{2,1,0:T(1,128)S(1)} %reshape.152), channel_id=1, replica_groups=mesh['sp'=8,'tp'=4] {'sp'}, dimensions={0}, use_global_device_ids=true | all-gather | bytes 13824 | tf_op jit(solution)/shard_map/all_gather | solution.py:154
  39.2 1.2 fusion.22
  40.3 32.1 %all_gather.23 = bf16[3072,64]{0,1:T(8,128)(2,1)S(1)} all-gather(bf16[384,64]{0,1:T(8,128)(2,1)S(1)} %pad_maximum_fusion), channel_id=1, replica_groups=mesh['sp'=8,'tp'=4] {'sp'}, dimensions={0}, use_global_device_ids=true | all-gather | bytes 442368 | tf_op jit(solution)/shard_map/all_gather | solution.py:153
  72.5 1.7 fusion.29
  74.2 0.7 broadcast_compare_fusion
  74.9 8.1 %fusion.31 = f32[3072,384,4]{0,1,2:T(8,128)} fusion(bf16[3072,64]{0,1:T(8,128)(2,1)S(1)} %all_gather.23, bf16[384,4,32]{0,2,1:T(8,128)(2,1)S(1)} %get-tuple-element.6, bf16[384,4,32]{0,2,1:T(8,128)(2,1)S(1)} %get-tuple-element.5), kind=kOutput, calls=%fused_computation.39 | convolution fusion | flops 604372992 | bytes 19464192 | tf_op jit(solution)/shard_map/qhd,kd->hqk/dot_general | solution.py:116
  83.0 2.4 convolution_convert_fusion.1
  85.5 12.7 %fusion.41 = (f32[4,384]{1,0:T(4,128)S(1)}, f32[4,384,3072]{2,1,0:T(8,128)}) fusion(f32[3072,384,4]{0,1,2:T(8,128)} %fusion.31, bf16[3072,4,128]{0,2,1:T(8,128)(2,1)S(1)} %bitcast.44, f32[384,4,192]{0,2,1:T(8,128)S(1)} %bitcast.47, pred[384,3072]{1,0:T(8,128)(4,1)S(1)} %broadcast_compare_fusion), kind=kOutput, calls=%fused_computation.67 | convolution fusion | flops 1226832384 | bytes 42473472 | tf_op jit(solution)/shard_map/qhd,khd->hqk/dot_general | solution.py:111
  98.2 9.0 %fusion.2 = f32[4,384]{1,0:T(4,128)S(1)} fusion(f32[4,384,3072]{2,1,0:T(8,128)} %get-tuple-element.16, f32[4,384]{1,0:T(4,128)S(1)} %get-tuple-element.10, pred[384,3072]{1,0:T(8,128)(4,1)S(1)} %broadcast_compare_fusion), kind=kLoop, calls=%fused_computation.4 | loop fusion | flops 14154240 | bytes 20066304 | tf_op jit(solution)/shard_map/reduce_sum | solution.py:123
  107.2 2.7 convolution_convert_fusion
  109.9 10.9 %fusion.19 = bf16[384,4,128]{0,2,1:T(8,128)(2,1)S(1)} fusion(bf16[3072,4,128]{0,2,1:T(8,128)(2,1)} %bitcast.45, f32[4,384,3072]{2,1,0:T(8,128)} %get-tuple-element.16, f32[4,384]{1,0:T(4,128)S(1)} %get-tuple-element.10, pred[384,3072]{1,0:T(8,128)(4,1)S(1)} %broadcast_compare_fusion, f32[384,4]{0,1:T(4,128)S(1)} %bitcast_add_fusion.1, ...), kind=kOutput, calls=%fused_computation.22 | convolution fusion | flops 1222705152 | bytes 23611392 | tf_op jit(solution)/shard_map/hqk,khd->qhd/dot_general | solution.py:124
  121.1 0.9 all_to_all.14
  122.0 3.5 all-to-all-start
  125.7 7.1 %all-to-all-done = bf16[4,96,512]{2,1,0:T(8,128)(2,1)S(1)} async-done(((bf16[4,96,512]{2,1,0:T(8,128)(2,1)}), bf16[4,96,512]{2,1,0:T(8,128)(2,1)S(1)}, u32[]{:S(2)}, u32[]{:S(2)}) %all-to-all-start) | async-done | bytes 393248 | tf_op jit(solution)/shard_map/all_to_all | solution.py:164
  132.9 5.0 %fusion.42 = (f32[96]{0:T(128)S(1)}, f32[96,2048]{1,0:T(8,128)S(1)}) fusion(bf16[96,2048]{1,0:T(8,128)(2,1)S(1)} %bitcast.48, bf16[2048,2048]{1,0:T(8,128)(2,1)} %param.26, bf16[384,2048]{1,0:T(8,128)(2,1)} %param.16, s32[]{:T(128)S(6)} %select_n.10), kind=kOutput, calls=%fused_computation.68 | convolution fusion | flops 806092672 | bytes 9961860 | tf_op jit(solution)/shard_map/dot_general | solution.py:165
  138.1 0.9 multiply_convert_fusion.1
  139.1 0.7 all-gather.11.cloned.1.call-update
  140.4 0.5 all-gather.15.cloned.1.call-update
  141.0 16.3 %all-gather.9.cloned.1.call-done = bf16[384,2048]{1,0:T(8,128)(2,1)} async-done(((bf16[96,2048]{1,0:T(8,128)(2,1)}), bf16[384,2048]{1,0:T(8,128)(2,1)}) %all-gather.9.cloned.1.call-update) | async-done | bytes 1572880 | tf_op jit(solution)/shard_map/all_gather | solution.py:170
  157.3 94.5 %all-gather.11.cloned.1.call-done = bf16[2048,1408]{1,0:T(8,128)(2,1)} async-done(((bf16[256,1408]{1,0:T(8,128)(2,1)}), bf16[2048,1408]{1,0:T(8,128)(2,1)}) %all-gather.11.cloned.1.call-update) | async-done | bytes 5767184 | tf_op jit(solution)/shard_map/all_gather | solution.py:173
  251.8 7.1 %fusion.43 = f32[384,1408]{1,0:T(8,128)} fusion(bf16[384,2048]{1,0:T(8,128)(2,1)} %all-gather.9.cloned.1.call-done, bf16[2048,1408]{1,0:T(8,128)(2,1)} %all-gather.11.cloned.1.call-done), kind=kOutput, calls=%fused_computation.69 | convolution fusion | flops 2214592512 | bytes 9502720 | tf_op jit(solution)/shard_map/dot_general | solution.py:171
  258.9 85.5 %all-gather.13.cloned.1.call-done = bf16[2048,1408]{1,0:T(8,128)(2,1)} async-done(((bf16[256,1408]{1,0:T(8,128)(2,1)}), bf16[2048,1408]{1,0:T(8,128)(2,1)}) %all-gather.13.cloned.1.call-update) | async-done | bytes 5767184 | tf_op jit(solution)/shard_map/all_gather | solution.py:178
  344.4 93.2 %all-gather.15.cloned.1.call-done = bf16[1408,2048]{1,0:T(8,128)(2,1)} async-done(((bf16[1408,256]{1,0:T(8,128)(2,1)}), bf16[1408,2048]{1,0:T(8,128)(2,1)}) %all-gather.15.cloned.1.call-update) | async-done | bytes 5767184 | tf_op jit(solution)/shard_map/all_gather | solution.py:183
  437.6 11.3 %convolution_convert_fusion.2 = bf16[384,2048]{1,0:T(8,128)(2,1)} fusion(bf16[1408,2048]{1,0:T(8,128)(2,1)} %all-gather.15.cloned.1.call-done, bf16[384,2048]{1,0:T(8,128)(2,1)S(1)} %copy-done.8, bf16[2048,1408]{1,0:T(8,128)(2,1)} %all-gather.13.cloned.1.call-done, f32[384,1408]{1,0:T(8,128)} %fusion.43), kind=kOutput, calls=%fused_computation.14 | convolution fusion | flops 4433215488 | bytes 16842752 | tf_op jit(solution)/shard_map/dot_general | solution.py:182
  448.9 26.4 %reduce-scatter.2.cloned.1.call-done = bf16[96,2048]{1,0:T(8,128)(2,1)} async-done(((bf16[384,2048]{1,0:T(8,128)(2,1)}), bf16[96,2048]{1,0:T(8,128)(2,1)}) %reduce-scatter.2.cloned.1.call-update) | async-done | bytes 393232 | tf_op jit(solution)/shard_map/reduce_scatter | solution.py:185
  475.3 1.4 fusion.25
  476.7 1.4 multiply_reduce_fusion
  478.2 2.2 multiply_convert_fusion
  (45 shorter events, 2.0 us)
Async XLA Ops:
  6.5 65.9 %copy-start = (bf16[512,768]{1,0:T(8,128)(2,1)S(1)}, bf16[512,768]{1,0:T(8,128)(2,1)}, u32[]{:S(2)}) copy-start(bf16[512,768]{1,0:T(8,128)(2,1)} %param.23) | copy-start | bytes 2359300
  6.5 67.7 %copy-start.7 = (s32[384]{0:T(512)S(1)}, s32[384]{0:T(512)}, u32[]{:S(2)}) copy-start(s32[384]{0:T(512)} %param.20) | copy-start | bytes 4612
  6.5 76.5 %all-gather.7.cloned.1.call-start = ((), (), s32[]{:S(2)}) async-start(), calls=%async_computation.2 | async-start | bytes 1769472 | tf_op jit(solution)/shard_map/all_gather | solution.py:152
  74.9 8.1 %copy-start.3 = (bf16[256,512]{1,0:T(8,128)(2,1)S(1)}, bf16[256,512]{1,0:T(8,128)(2,1)}, u32[]{:S(2)}) copy-start(bf16[256,512]{1,0:T(8,128)(2,1)} %param.24) | copy-start | bytes 786436
  98.2 9.1 %copy-start.2 = (bf16[3072,256]{1,0:T(8,128)(2,1)S(1)}, bf16[3072,256]{1,0:T(8,128)(2,1)}, u32[]{:S(2)}) copy-start(bf16[3072,256]{1,0:T(8,128)(2,1)} %all-gather.7.cloned.1.call-done) | copy-start | bytes 4718596
  98.2 9.1 %copy-start.4 = (bf16[256,512]{1,0:T(8,128)(2,1)S(1)}, bf16[256,512]{1,0:T(8,128)(2,1)}, u32[]{:S(2)}) copy-start(bf16[256,512]{1,0:T(8,128)(2,1)} %param.25) | copy-start | bytes 786436
  122.0 10.8 %all-to-all-start = ((bf16[4,96,512]{2,1,0:T(8,128)(2,1)}), bf16[4,96,512]{2,1,0:T(8,128)(2,1)S(1)}, u32[]{:S(2)}, u32[]{:S(2)}) async-start(bf16[4,96,512]{2,1,0:T(8,128)(2,1)} %all_to_all.14), calls=%async_computation | async-start | bytes 786432 | tf_op jit(solution)/shard_map/all_to_all | solution.py:164
  125.4 31.8 %all-gather.9.cloned.1.call-start = ((), (), s32[]{:S(2)}) async-start(), calls=%async_computation.3 | async-start | bytes 1966080 | tf_op jit(solution)/shard_map/all_gather | solution.py:170
  132.8 5.3 %copy-start.5 = (f32[2048]{0:T(1024)S(1)}, f32[2048]{0:T(1024)}, u32[]{:S(2)}) copy-start(f32[2048]{0:T(1024)} %param.27) | copy-start | bytes 24580
  139.1 112.8 %all-gather.11.cloned.1.call-start = ((), (), s32[]{:S(2)}) async-start(), calls=%async_computation.4 | async-start | bytes 6488064 | tf_op jit(solution)/shard_map/all_gather | solution.py:173
  139.8 204.6 %all-gather.13.cloned.1.call-start = ((), (), s32[]{:S(2)}) async-start(), calls=%async_computation.5 | async-start | bytes 6488064 | tf_op jit(solution)/shard_map/all_gather | solution.py:178
  140.4 297.2 %all-gather.15.cloned.1.call-start = ((), (), s32[]{:S(2)}) async-start(), calls=%async_computation.6 | async-start | bytes 6488064 | tf_op jit(solution)/shard_map/all_gather | solution.py:183
  141.0 334.4 %reduce-scatter.2.cloned.1.call-start = ((), (), s32[]{:S(2)}) async-start(), calls=%async_computation.7 | async-start | bytes 1966080 | tf_op jit(solution)/shard_map/reduce_scatter | solution.py:185
  157.3 280.3 %copy-start.8 = (bf16[384,2048]{1,0:T(8,128)(2,1)S(1)}, bf16[384,2048]{1,0:T(8,128)(2,1)}, u32[]{:S(2)}) copy-start(bf16[384,2048]{1,0:T(8,128)(2,1)} %all-gather.9.cloned.1.call-done) | copy-start | bytes 4718596
  437.6 42.8 %copy-start.1 = (bf16[512,768]{1,0:T(8,128)(2,1)S(1)}, bf16[512,768]{1,0:T(8,128)(2,1)}, u32[]{:S(2)}) copy-start(bf16[512,768]{1,0:T(8,128)(2,1)} %param.23) | copy-start | bytes 2359300
  448.9 29.3 %copy-start.6 = (f32[2048]{0:T(1024)S(1)}, f32[2048]{0:T(1024)}, u32[]{:S(2)}) copy-start(f32[2048]{0:T(1024)} %param.31) | copy-start | bytes 24580
Sparse Core Ops, SparseCore 0:
  9.6 49.9 all-gather.6
  139.2 18.0 all-gather.8
  159.5 92.3 all-gather.10
  253.8 90.4 all-gather.12
  346.3 91.2 all-gather.14
  449.1 26.2 reduce-scatter.1
where the time goes:
time: 488 us; the launch traced here: 487 us
  waiting for transfers between devices  325 us (67%)
  matrix products  61.8 us (13%)
  blocking collectives  60 us (12%)
  other arithmetic  21.1 us (4%)
  between operations  13.7 us (3%)
    all_gather x1, waiting for transfers between devices, body(): lax.all_gather(w_gate, 'sp', axis=0, tiled=True)  94.5 us
    all_gather x1, waiting for transfers between devices, body(): lax.all_gather(w_down, 'sp', axis=1, tiled=True)  93.2 us
    all_gather x1, waiting for transfers between devices, body(): lax.all_gather(w_up, 'sp', axis=0, tiled=True)  85.5 us
    all_gather x1, blocking collectives, body(): lax.all_gather(key_rot, 'sp', axis=0, tiled=True)  32.1 us
    all_gather x1, blocking collectives, body(): lax.all_gather(doc_ids, 'sp', axis=0, tiled=True)  27.9 us
    reduce_scatter x1, waiting for transfers between devices, body(): lax.psum_scatter(down_term.astype(jnp.bfloat16), 'tp', scatter_dimension=...  26.4 us
    all_gather x1, waiting for transfers between devices, body(): normed_rows = lax.all_gather(own_normed, 'tp', axis=0, tiled=True)  16.3 us
    dot_general x1, matrix products, attend_rows(): jnp.einsum('qhd,khd->hqk', query_nope, keys_heads, preferred_element_type...  12.7 us
  transfers between devices with their start and end apart: 7, of which 6 were waited for; matrix products, arithmetic and copies ran while one was open for 4% of the time, Pallas kernels for 0%

commit v1 on v0

--- a/solution.py
+++ b/solution.py
@@ -63,6 +63,54 @@
         outcome = lax.scan(one_block, carried, jnp.arange(piece_rows // key_span, dtype=jnp.int32))
         return outcome[0]
     return attend_fn(carried, piece_part)
+
+
+class Ring:
+    def __init__(self, blocks):
+        self.count = lax.axis_size("sp")
+        ring = list(range(0, self.count, 2)) + list(range(1, self.count, 2))[::-1]
+        places = [ring.index(i) for i in range(self.count)]
+        self.place = jnp.array(places, jnp.int32)[lax.axis_index("sp")]
+        self.ring_of = jnp.array(ring, jnp.int32)
+        self.right = [(ring[i], ring[(i + 1) % self.count]) for i in range(self.count)]
+        self.left = [(after, before) for before, after in self.right]
+        self.pieces = [[(lax.axis_index("sp"), block)] for block in blocks]
+        self.flying = [(block, block) for block in blocks]
+        self.step = 0
+
+    def owner(self, distance):
+        return self.ring_of[(self.place + distance) % self.count]
+
+    def hop(self):
+        self.step += 1
+        self.send()
+
+    def send(self):
+        if self.step < self.count // 2:
+            self.flying = [
+                (lax.ppermute(one, "sp", self.right), lax.ppermute(two, "sp", self.left))
+                for one, two in self.flying
+            ]
+        elif self.step == self.count // 2:
+            self.flying = [
+                (
+                    lax.ppermute(one[: one.shape[0] // 2], "sp", self.right),
+                    lax.ppermute(two[two.shape[0] // 2 :], "sp", self.left),
+                )
+                for one, two in self.flying
+            ]
+
+    def land(self, *values):
+        if self.step <= self.count // 2:
+            if values:
+                values, self.flying = lax.optimization_barrier((values, self.flying))
+            for pieces, (one, two) in zip(self.pieces, self.flying):
+                if self.step < self.count // 2:
+                    pieces.append((self.owner(-self.step), one))
+                    pieces.append((self.owner(self.step), two))
+                else:
+                    pieces.append((self.owner(self.step), jnp.concatenate([one, two])))
+        return values
 
 
 def body(
@@ -88,6 +136,8 @@
     tp_count = lax.axis_size("tp")
     part_rows = tok_rows // tp_count
     tp_index = lax.axis_index("tp")
+    ring = Ring([jnp.concatenate([w_gate, w_up], axis=1), w_down])
+    ring.hop()
     positions = lax.axis_index("sp") * tok_rows + jnp.arange(tok_rows, dtype=jnp.int32)
     cos_table, sin_table = rope_angles(positions)
     q_normed = rms_scaled(q_latent, q_gain)
@@ -102,7 +152,7 @@
     key_rot = rotate(rope_key.astype(jnp.float32), cos_table, sin_table).astype(jnp.bfloat16)
     score_scale = (NOPE + RD) ** (-0.5)
 
-    def attend_rows(carried, piece_part):
+    def attend_rows(carried, piece_part, between=lambda value: value):
         row_top, denom_sum, accum_out = carried
         key_piece, value_piece, rot_piece, doc_piece = piece_part
         piece_rows = key_piece.shape[0]
@@ -121,11 +171,9 @@
         weights = jnp.where(same_doc, jnp.exp(masked - new_top[:, :, None]), 0.0)
         factor = jnp.exp(row_top - new_top)
         denom_sum = denom_sum * factor + jnp.sum(weights, axis=-1)
+        weights = between(weights.astype(jnp.bfloat16))
         update = jnp.einsum(
-            "hqk,khd->qhd",
-            weights.astype(jnp.bfloat16),
-            values_heads,
-            preferred_element_type=jnp.float32,
+            "hqk,khd->qhd", weights, values_heads, preferred_element_type=jnp.float32
         )
         accum_out = accum_out * jnp.transpose(factor)[:, :, None] + update
         return (new_top, denom_sum, accum_out)
@@ -136,7 +184,7 @@
         jnp.zeros((tok_rows, head_count, VD), jnp.float32),
     )
 
-    def project_rows(carried, piece_part):
+    def project_rows(carried, piece_part, between=lambda value: value):
         latent_piece, rot_piece, doc_piece = piece_part
         key_piece = jnp.dot(latent_piece, w_key, preferred_element_type=jnp.float32).astype(
             jnp.bfloat16
@@ -144,17 +192,27 @@
         value_piece = jnp.dot(latent_piece, w_value, preferred_element_type=jnp.float32).astype(
             jnp.bfloat16
         )
-        return attend_rows(carried, (key_piece, value_piece, rot_piece, doc_piece))
-
-    carried_out = fold_in_blocks(
-        initial,
-        (
-            lax.all_gather(kv_normed, "sp", axis=0, tiled=True),
-            lax.all_gather(key_rot, "sp", axis=0, tiled=True),
-            lax.all_gather(doc_ids, "sp", axis=0, tiled=True),
-        ),
-        project_rows,
-    )
+        return attend_rows(carried, (key_piece, value_piece, rot_piece, doc_piece), between)
+
+    def next_hop(value):
+        (value,) = ring.land(value)
+        ring.hop()
+        return value
+
+    doc_lanes = jnp.broadcast_to(doc_ids.astype(jnp.bfloat16)[:, None], (tok_rows, RD))
+    packed = jnp.concatenate([kv_normed, key_rot, doc_lanes], axis=1)
+    packed_all = lax.all_gather(packed, "sp", axis=0, tiled=True)
+    packed_all = next_hop(packed_all)
+    kv_rank = kv_latent.shape[1]
+    gathered = (
+        packed_all[:, :kv_rank],
+        packed_all[:, kv_rank : kv_rank + RD],
+        packed_all[:, kv_rank + RD].astype(jnp.int32),
+    )
+    if packed_all.shape[0] > key_span and packed_all.shape[0] % key_span == 0:
+        carried_out = fold_in_blocks(initial, gathered, project_rows)
+    else:
+        carried_out = project_rows(initial, gathered, next_hop)
     denom_sum = carried_out[1]
     attended = (
         (carried_out[2] / jnp.transpose(denom_sum)[:, :, None])
@@ -167,24 +225,38 @@
     own_normed = layer_scaled(
         resid_alpha * own_resid.astype(jnp.float32) + mixer_out, mix_gain
     ).astype(jnp.bfloat16)
+    own_normed = next_hop(own_normed)
     normed_rows = lax.all_gather(own_normed, "tp", axis=0, tiled=True)
-    gate_part = jnp.dot(
-        normed_rows,
-        lax.all_gather(w_gate, "sp", axis=0, tiled=True),
-        preferred_element_type=jnp.float32,
-    )
-    up_part = jnp.dot(
-        normed_rows,
-        lax.all_gather(w_up, "sp", axis=0, tiled=True),
-        preferred_element_type=jnp.float32,
-    )
-    hidden = (jax.nn.silu(gate_part) * up_part).astype(jnp.bfloat16)
-    down_term = jnp.dot(
-        hidden, lax.all_gather(w_down, "sp", axis=1, tiled=True), preferred_element_type=jnp.float32
-    )
-    ffn_sum = lax.psum_scatter(
-        down_term.astype(jnp.bfloat16), "tp", scatter_dimension=0, tiled=True
-    ).astype(jnp.float32)
+    ring.land()
+    while ring.step < ring.count // 2:
+        ring.hop()
+        ring.land()
+    gate_up, down = ring.pieces
+    gate_sum = None
+    for owner, piece in gate_up:
+        rows = lax.dynamic_slice_in_dim(normed_rows, owner * piece.shape[0], piece.shape[0], 1)
+        term = jnp.dot(rows, piece, preferred_element_type=jnp.float32)
+        gate_sum = term if gate_sum is None else gate_sum + term
+    width = w_gate.shape[1]
+    hidden = (jax.nn.silu(gate_sum[:, :width]) * gate_sum[:, width:]).astype(jnp.bfloat16)
+    ffn_sum = jnp.zeros((part_rows, resid_stream.shape[1]), jnp.float32)
+    for group in (down[: len(down) // 2], down[len(down) // 2 :]):
+        partial = jnp.concatenate(
+            [
+                jnp.dot(hidden, piece, preferred_element_type=jnp.float32).astype(jnp.bfloat16)
+                for _, piece in group
+            ],
+            axis=1,
+        )
+        swapped = lax.all_to_all(
+            partial.reshape(tp_count, part_rows, -1), "tp", split_axis=0, concat_axis=0, tiled=True
+        )
+        summed = jnp.sum(swapped.astype(jnp.float32), axis=0)
+        columns = w_down.shape[1]
+        for at, (owner, _) in enumerate(group):
+            ffn_sum = lax.dynamic_update_slice_in_dim(
+                ffn_sum, summed[:, at * columns : (at + 1) * columns], owner * columns, 1
+            )
     layer_out = layer_scaled(
         resid_alpha * own_normed.astype(jnp.float32) + 0.5 * ffn_sum, out_gain
     ).astype(jnp.bfloat16)

time: 488 us -> 312 us (0.64)
  waiting for transfers between devices: 325 us -> 165 us
  blocking collectives: 60 us -> 0 us
  starting transfers between devices: 3.88 us -> 27.9 us
  local copies, waits for them, and re-layouts: 1.9 us -> 17.3 us
  between operations: 13.7 us -> 22.5 us
    all_gather x4 -> x1, waiting for transfers between devices: 273 us -> 0.01 us  [body(): packed_all = lax.all_gather(packed, 'sp', axis=0, tiled=True)]
    ppermute x0 -> x16, waiting for transfers between devices: none -> 144 us  [the longest x6 137 us: send(): lax.ppermute(one, 'sp', self.right)]
    all_gather x2 -> x0, blocking collectives: 60 us -> none  [the longest x1 32.1 us: body(): lax.all_gather(key_rot, 'sp', axis=0, tiled=True)]
    reduce_scatter x1 -> x0, waiting for transfers between devices: 26.4 us -> none  [body(): lax.psum_scatter(down_term.astype(jnp.bfloat16), 'tp', scatter_dimension=...]
    all_to_all x0 -> x2, waiting for transfers between devices: none -> 17.5 us  [body(): lax.all_to_all(partial.reshape(tp_count, part_rows, -1), 'tp', split_axis...]
    ppermute x0 -> x16, starting transfers between devices: none -> 17.4 us  [the longest x6 12.1 us: send(): lax.ppermute(one, 'sp', self.right)]
    all_gather x1, waiting for transfers between devices: 16.3 us -> 0.01 us  [body(): normed_rows = lax.all_gather(own_normed, 'tp', axis=0, tiled=True)]
    all_to_all x0 -> x2, starting transfers between devices: none -> 6.99 us  [body(): lax.all_to_all(partial.reshape(tp_count, part_rows, -1), 'tp', split_axis...]
  transfers between devices with their start and end apart: 7 -> 21, of which waited for: 6 -> 10; matrix products, arithmetic and copies ran while one was open for 4% -> 16% of each run, Pallas kernels for 0% -> 0%
where the time goes in v1:
time: 312 us; the launch traced here: 311 us
  waiting for transfers between devices  165 us (53%)
  matrix products  57.2 us (18%)
  starting transfers between devices  27.9 us (9%)
  between operations  22.5 us (7%)
  other arithmetic  21.9 us (7%)
  local copies, waits for them, and re-layouts  17.3 us (6%)
    ppermute x6, waiting for transfers between devices, send(): lax.ppermute(one, 'sp', self.right)  137 us
    all_to_all x2, waiting for transfers between devices, body(): lax.all_to_all(partial.reshape(tp_count, part_rows, -1), 'tp', split_axis...  17.5 us
    dot_general x1, matrix products, attend_rows(): jnp.einsum('qhd,khd->hqk', query_nope, keys_heads, preferred_element_type...  12.9 us
    reduce_sum x1, other arithmetic, attend_rows(): denom_sum = denom_sum * factor + jnp.sum(weights, axis=-1)  12.9 us
    dot_general x8, matrix products, body(): term = jnp.dot(rows, piece, preferred_element_type=jnp.float32)  12.2 us
    ppermute x6, starting transfers between devices, send(): lax.ppermute(one, 'sp', self.right)  12.1 us
    dot_general x8, matrix products, body(): jnp.dot(hidden, piece, preferred_element_type=jnp.float32)  8.29 us
    dot_general x1, matrix products, attend_rows(): jnp.einsum('qhd,kd->hqk', query_rope, rot_piece, preferred_element_type=j...  7.88 us
  transfers between devices with their start and end apart: 21, of which 10 were waited for; matrix products, arithmetic and copies ran while one was open for 16% of the time, Pallas kernels for 0%

profile of v1, /device:TPU:0, one launch (start us, length us, event | category | flops | bytes accessed | tf_op | source)
XLA Modules:
  0.0 311.3 jit_solution(11948798122179735957)
XLA Ops:
  11.5 3.1 collective-permute-start
  14.6 2.0 collective-permute-start.2
  18.6 70.2 %collective-permute-done.2 = bf16[1408,256]{1,0:T(8,128)(2,1)S(1)} collective-permute-done((bf16[1408,256]{1,0:T(8,128)(2,1)S(1)}, bf16[1408,256]{1,0:T(8,128)(2,1)S(1)}, u32[]{:S(2)}, u32[]{:S(2)}) %collective-permute-start.2) | collective-permute-done | bytes 720928 | tf_op jit(solution)/shard_map/ppermute | solution.py:91
  88.8 2.5 collective-permute-done.3
  94.1 2.6 convolution_convert_fusion.1
  96.7 7.9 %fusion.30 = f32[3072,384,4]{0,1,2:T(8,128)} fusion(bf16[3072,384]{0,1:T(8,128)(2,1)S(1)} %copy-done.2, bf16[384,4,32]{0,2,1:T(8,128)(2,1)S(1)} %get-tuple-element.38, bf16[384,4,32]{0,2,1:T(8,128)(2,1)S(1)} %get-tuple-element.37), kind=kOutput, calls=%fused_computation.60 | convolution fusion | flops 604372992 | bytes 19464192 | tf_op jit(solution)/shard_map/qhd,kd->hqk/dot_general | solution.py:166
  104.5 12.9 %fusion.64 = (f32[4,384]{1,0:T(4,128)S(1)}, f32[4,384,3072]{2,1,0:T(8,128)}) fusion(f32[3072,384,4]{0,1,2:T(8,128)} %fusion.30, bf16[3072,4,128]{0,2,1:T(8,128)(2,1)S(1)} %bitcast.76, f32[384,4,192]{0,2,1:T(8,128)} %bitcast.79, pred[384,3072]{1,0:T(8,128)(4,1)S(1)} %broadcast_compare_fusion), kind=kOutput, calls=%fused_computation.123 | convolution fusion | flops 1226832384 | bytes 42473472 | tf_op jit(solution)/shard_map/qhd,khd->hqk/dot_general | solution.py:161
  117.5 1.8 collective-permute-start.4
  119.6 1.7 collective-permute-start.6
  121.6 12.9 %fusion.2 = (f32[4,384]{1,0:T(4,128)S(1)}, bf16[4,384,3072]{2,1,0:T(8,128)(2,1)}) fusion(f32[4,384,3072]{2,1,0:T(8,128)} %get-tuple-element.55, f32[4,384]{1,0:T(4,128)S(1)} %get-tuple-element.42, pred[384,3072]{1,0:T(8,128)(4,1)S(1)} %broadcast_compare_fusion), kind=kLoop, calls=%fused_computation.4 | loop fusion | flops 18872832 | bytes 29503488 | tf_op jit(solution)/shard_map/reduce_sum | solution.py:173
  135.6 30.3 %collective-permute-done.6 = bf16[1408,256]{1,0:T(8,128)(2,1)} collective-permute-done((bf16[1408,256]{1,0:T(8,128)(2,1)S(1)}, bf16[1408,256]{1,0:T(8,128)(2,1)}, u32[]{:S(2)}, u32[]{:S(2)}) %collective-permute-start.6) | collective-permute-done | bytes 720928 | tf_op jit(solution)/shard_map/ppermute | solution.py:91
  168.8 6.6 %fusion.18 = bf16[384,4,128]{0,2,1:T(8,128)(2,1)S(1)} fusion(bf16[3072,4,128]{0,2,1:T(8,128)(2,1)S(1)} %bitcast.77, bf16[4,384,3072]{2,1,0:T(8,128)(2,1)} %get-tuple-element.25, f32[384,4]{0,1:T(4,128)S(1)} %bitcast_add_fusion.1, f32[384,4]{0,1:T(4,128)S(1)} %get-tuple-element.41), kind=kOutput, calls=%fused_computation.29 | convolution fusion | flops 1208549376 | bytes 12988416 | tf_op jit(solution)/shard_map/hqk,khd->qhd/dot_general | solution.py:175
  176.5 3.5 %all-to-all-start = ((bf16[4,96,512]{2,1,0:T(8,128)(2,1)}), bf16[4,96,512]{2,1,0:T(8,128)(2,1)S(1)}, u32[]{:S(2)}, u32[]{:S(2)}) async-start(bf16[4,96,512]{2,1,0:T(8,128)(2,1)} %all_to_all.20), calls=%async_computation | async-start | bytes 786432 | tf_op jit(solution)/shard_map/all_to_all | solution.py:222
  180.0 1.8 collective-permute-start.8
  182.1 1.7 collective-permute-start.10
  184.2 3.2 %all-to-all-done = bf16[4,96,512]{2,1,0:T(8,128)(2,1)S(1)} async-done(((bf16[4,96,512]{2,1,0:T(8,128)(2,1)}), bf16[4,96,512]{2,1,0:T(8,128)(2,1)S(1)}, u32[]{:S(2)}, u32[]{:S(2)}) %all-to-all-start) | async-done | bytes 393248 | tf_op jit(solution)/shard_map/all_to_all | solution.py:222
  187.4 5.0 %fusion.65 = (f32[96]{0:T(128)S(1)}, f32[96,2048]{1,0:T(8,128)S(1)}) fusion(bf16[96,2048]{1,0:T(8,128)(2,1)S(1)} %bitcast.80, bf16[2048,2048]{1,0:T(8,128)(2,1)} %param.28, bf16[384,2048]{1,0:T(8,128)(2,1)} %param.18, s32[]{:T(128)S(6)} %select_n.118), kind=kOutput, calls=%fused_computation.124 | convolution fusion | flops 806092672 | bytes 9961860 | tf_op jit(solution)/shard_map/dot_general | solution.py:223
  193.6 36.1 %collective-permute-done.10 = bf16[1408,256]{1,0:T(8,128)(2,1)} collective-permute-done((bf16[1408,256]{1,0:T(8,128)(2,1)}, bf16[1408,256]{1,0:T(8,128)(2,1)}, u32[]{:S(2)}, u32[]{:S(2)}) %collective-permute-start.10) | collective-permute-done | bytes 720928 | tf_op jit(solution)/shard_map/ppermute | solution.py:91
  242.1 2.1 slice.79
  248.0 1.6 collective-permute-start.15
  249.6 2.3 fusion.39
  252.0 2.2 fusion.49
  258.4 2.7 fusion.6
  261.2 2.3 collective-permute-done.13
  263.5 1.9 add_add_fusion
  268.9 1.7 convolution_convert_fusion.6
  272.5 3.5 %all-to-all-start.1 = ((bf16[4,96,1024]{2,1,0:T(8,128)(2,1)}), bf16[4,96,1024]{2,1,0:T(8,128)(2,1)S(1)}, u32[]{:S(2)}, u32[]{:S(2)}) async-start(bf16[4,96,1024]{2,1,0:T(8,128)(2,1)} %bitcast.24), calls=%async_computation.1 | async-start | bytes 1572864 | tf_op jit(solution)/shard_map/all_to_all | solution.py:251
  276.0 1.7 convolution_convert_fusion.4
  277.8 1.7 convolution_convert_fusion.2
  281.4 6.2 %all-to-all-done.1 = bf16[4,96,1024]{2,1,0:T(8,128)(2,1)S(1)} async-done(((bf16[4,96,1024]{2,1,0:T(8,128)(2,1)}), bf16[4,96,1024]{2,1,0:T(8,128)(2,1)S(1)}, u32[]{:S(2)}, u32[]{:S(2)}) %all-to-all-start.1) | async-done | bytes 786464 | tf_op jit(solution)/shard_map/all_to_all | solution.py:251
  287.6 3.5 %all-to-all-start.2 = ((bf16[4,96,1024]{2,1,0:T(8,128)(2,1)}), bf16[4,96,1024]{2,1,0:T(8,128)(2,1)S(1)}, u32[]{:S(2)}, u32[]{:S(2)}) async-start(bf16[4,96,1024]{2,1,0:T(8,128)(2,1)} %bitcast.25), calls=%async_computation.2 | async-start | bytes 1572864 | tf_op jit(solution)/shard_map/all_to_all | solution.py:251
  291.4 11.3 %all-to-all-done.2 = bf16[4,96,1024]{2,1,0:T(8,128)(2,1)S(1)} async-done(((bf16[4,96,1024]{2,1,0:T(8,128)(2,1)}), bf16[4,96,1024]{2,1,0:T(8,128)(2,1)S(1)}, u32[]{:S(2)}, u32[]{:S(2)}) %all-to-all-start.2) | async-done | bytes 786464 | tf_op jit(solution)/shard_map/all_to_all | solution.py:251
  (158 shorter events, 38.2 us)
Async XLA Ops:
  6.5 10.2 %copy-start = (bf16[512,768]{1,0:T(8,128)(2,1)S(1)}, bf16[512,768]{1,0:T(8,128)(2,1)}, u32[]{:S(2)}) copy-start(bf16[512,768]{1,0:T(8,128)(2,1)} %param.25) | copy-start | bytes 2359300
  6.5 86.0 %all-gather.3.cloned.1.call-start = ((), (), s32[]{:S(2)}) async-start(), calls=%async_computation.3 | async-start | bytes 2654208 | tf_op jit(solution)/shard_map/all_gather | solution.py:204
  11.3 5.5 %copy-start.32 = (f32[512]{0:T(512)S(1)}, f32[512]{0:T(512)}, u32[]{:S(2)}) copy-start(f32[512]{0:T(512)} %param.23) | copy-start | bytes 6148
  11.4 7.1 %copy-start.5 = (bf16[256,2816]{1,0:T(8,128)(2,1)}, bf16[256,2816]{1,0:T(8,128)(2,1)S(1)}, u32[]{:S(2)}) copy-start(bf16[256,2816]{1,0:T(8,128)(2,1)S(1)} %constant_dynamic-update-slice_fusion) | copy-start | bytes 4325380
  11.5 79.9 %collective-permute-start = (bf16[256,2816]{1,0:T(8,128)(2,1)S(1)}, bf16[256,2816]{1,0:T(8,128)(2,1)S(1)}, u32[]{:S(2)}, u32[]{:S(2)}) collective-permute-start(bf16[256,2816]{1,0:T(8,128)(2,1)S(1)} %constant_dynamic-update-slice_fusion), channel_id=1, source_target_pairs={{0,8},{8,16},{16,24},{24,28},{28,20},{20,12},{12,4},{4,0},{1,9},{9... | collective-permute-start | bytes 4325384 | tf_op jit(solution)/shard_map/ppermute | solution.py:91
  14.6 78.0 %collective-permute-start.1 = (bf16[256,2816]{1,0:T(8,128)(2,1)S(1)}, bf16[256,2816]{1,0:T(8,128)(2,1)}, u32[]{:S(2)}, u32[]{:S(2)}) collective-permute-start(bf16[256,2816]{1,0:T(8,128)(2,1)S(1)} %constant_dynamic-update-slice_fusion), channel_id=1, source_target_pairs={{8,0},{16,8},{24,16},{28,24},{20,28},{12,20},{4,12},{0,4},{9,1},{1... | collective-permute-start | bytes 4325384 | tf_op jit(solution)/shard_map/ppermute | solution.py:91
  14.6 74.3 %collective-permute-start.2 = (bf16[1408,256]{1,0:T(8,128)(2,1)S(1)}, bf16[1408,256]{1,0:T(8,128)(2,1)S(1)}, u32[]{:S(2)}, u32[]{:S(2)}) collective-permute-start(bf16[1408,256]{1,0:T(8,128)(2,1)S(1)} %copy-done.16), channel_id=1, source_target_pairs={{0,8},{8,16},{16,24},{24,28},{28,20},{20,12},{12,4},{4,0},{1,9},{9... | collective-permute-start | bytes 2162696 | tf_op jit(solution)/shard_map/ppermute | solution.py:91
  16.6 74.8 %collective-permute-start.3 = (bf16[1408,256]{1,0:T(8,128)(2,1)S(1)}, bf16[1408,256]{1,0:T(8,128)(2,1)S(1)}, u32[]{:S(2)}, u32[]{:S(2)}) collective-permute-start(bf16[1408,256]{1,0:T(8,128)(2,1)S(1)} %copy-done.16), channel_id=1, source_target_pairs={{8,0},{16,8},{24,16},{28,24},{20,28},{12,20},{4,12},{0,4},{9,1},{1... | collective-permute-start | bytes 2162696 | tf_op jit(solution)/shard_map/ppermute | solution.py:91
  16.8 76.6 %copy-start.31 = (s32[384]{0:T(512)S(1)}, s32[384]{0:T(512)}, u32[]{:S(2)}) copy-start(s32[384]{0:T(512)} %param.22) | copy-start | bytes 4612
  17.5 76.5 %copy-start.26 = (bf16[256,512]{1,0:T(8,128)(2,1)S(1)}, bf16[256,512]{1,0:T(8,128)(2,1)}, u32[]{:S(2)}) copy-start(bf16[256,512]{1,0:T(8,128)(2,1)} %param.26) | copy-start | bytes 786436
  104.5 15.0 %copy-start.19 = (bf16[1408,256]{1,0:T(8,128)(2,1)S(1)}, bf16[1408,256]{1,0:T(8,128)(2,1)}, u32[]{:S(2)}) copy-start(bf16[1408,256]{1,0:T(8,128)(2,1)} %copy-done.18) | copy-start | bytes 2162692
  104.5 16.7 %copy-start.22 = (bf16[1408,256]{1,0:T(8,128)(2,1)S(1)}, bf16[1408,256]{1,0:T(8,128)(2,1)}, u32[]{:S(2)}) copy-start(bf16[1408,256]{1,0:T(8,128)(2,1)} %copy-done.21) | copy-start | bytes 2162692
  117.5 49.4 %collective-permute-start.4 = (bf16[256,2816]{1,0:T(8,128)(2,1)}, bf16[256,2816]{1,0:T(8,128)(2,1)S(1)}, u32[]{:S(2)}, u32[]{:S(2)}) collective-permute-start(bf16[256,2816]{1,0:T(8,128)(2,1)} %copy-done.8), channel_id=1, source_target_pairs={{0,8},{8,16},{16,24},{24,28},{28,20},{20,12},{12,4},{4,0},{1,9},{9... | collective-permute-start | bytes 4325384 | tf_op jit(solution)/shard_map/ppermute | solution.py:91
  119.3 47.7 %collective-permute-start.5 = (bf16[256,2816]{1,0:T(8,128)(2,1)}, bf16[256,2816]{1,0:T(8,128)(2,1)S(1)}, u32[]{:S(2)}, u32[]{:S(2)}) collective-permute-start(bf16[256,2816]{1,0:T(8,128)(2,1)} %collective-permute-done.1), channel_id=1, source_target_pairs={{8,0},{16,8},{24,16},{28,24},{20,28},{12,20},{4,12},{0,4},{9,1},{1... | collective-permute-start | bytes 4325384 | tf_op jit(solution)/shard_map/ppermute | solution.py:91
  119.6 46.3 %collective-permute-start.6 = (bf16[1408,256]{1,0:T(8,128)(2,1)S(1)}, bf16[1408,256]{1,0:T(8,128)(2,1)}, u32[]{:S(2)}, u32[]{:S(2)}) collective-permute-start(bf16[1408,256]{1,0:T(8,128)(2,1)S(1)} %copy-done.19), channel_id=1, source_target_pairs={{0,8},{8,16},{16,24},{24,28},{28,20},{20,12},{12,4},{4,0},{1,9},{9... | collective-permute-start | bytes 2162696 | tf_op jit(solution)/shard_map/ppermute | solution.py:91
  121.3 45.7 %collective-permute-start.7 = (bf16[1408,256]{1,0:T(8,128)(2,1)S(1)}, bf16[1408,256]{1,0:T(8,128)(2,1)S(1)}, u32[]{:S(2)}, u32[]{:S(2)}) collective-permute-start(bf16[1408,256]{1,0:T(8,128)(2,1)S(1)} %copy-done.22), channel_id=1, source_target_pairs={{8,0},{16,8},{24,16},{28,24},{20,28},{12,20},{4,12},{0,4},{9,1},{1... | collective-permute-start | bytes 2162696 | tf_op jit(solution)/shard_map/ppermute | solution.py:91
  121.6 12.9 %copy-start.27 = (bf16[256,512]{1,0:T(8,128)(2,1)S(1)}, bf16[256,512]{1,0:T(8,128)(2,1)}, u32[]{:S(2)}) copy-start(bf16[256,512]{1,0:T(8,128)(2,1)} %param.27) | copy-start | bytes 786436
  176.5 10.8 %all-to-all-start = ((bf16[4,96,512]{2,1,0:T(8,128)(2,1)}), bf16[4,96,512]{2,1,0:T(8,128)(2,1)S(1)}, u32[]{:S(2)}, u32[]{:S(2)}) async-start(bf16[4,96,512]{2,1,0:T(8,128)(2,1)} %all_to_all.20), calls=%async_computation | async-start | bytes 786432 | tf_op jit(solution)/shard_map/all_to_all | solution.py:222
  180.0 69.6 %all-gather.5.cloned.1.call-start = ((), (), s32[]{:S(2)}) async-start(), calls=%async_computation.4 | async-start | bytes 1966080 | tf_op jit(solution)/shard_map/all_gather | solution.py:229
  180.0 51.0 %collective-permute-start.8 = (bf16[256,2816]{1,0:T(8,128)(2,1)}, bf16[256,2816]{1,0:T(8,128)(2,1)S(1)}, u32[]{:S(2)}, u32[]{:S(2)}) collective-permute-start(bf16[256,2816]{1,0:T(8,128)(2,1)} %copy-done.10), channel_id=1, source_target_pairs={{0,8},{8,16},{16,24},{24,28},{28,20},{20,12},{12,4},{4,0},{1,9},{9... | collective-permute-start | bytes 4325384 | tf_op jit(solution)/shard_map/ppermute | solution.py:91
  181.8 49.2 %collective-permute-start.9 = (bf16[256,2816]{1,0:T(8,128)(2,1)}, bf16[256,2816]{1,0:T(8,128)(2,1)}, u32[]{:S(2)}, u32[]{:S(2)}) collective-permute-start(bf16[256,2816]{1,0:T(8,128)(2,1)} %copy-done.12), channel_id=1, source_target_pairs={{8,0},{16,8},{24,16},{28,24},{20,28},{12,20},{4,12},{0,4},{9,1},{1... | collective-permute-start | bytes 4325384 | tf_op jit(solution)/shard_map/ppermute | solution.py:91
  182.1 47.6 %collective-permute-start.10 = (bf16[1408,256]{1,0:T(8,128)(2,1)}, bf16[1408,256]{1,0:T(8,128)(2,1)}, u32[]{:S(2)}, u32[]{:S(2)}) collective-permute-start(bf16[1408,256]{1,0:T(8,128)(2,1)} %collective-permute-done.6), channel_id=1, source_target_pairs={{0,8},{8,16},{16,24},{24,28},{28,20},{20,12},{12,4},{4,0},{1,9},{9... | collective-permute-start | bytes 2162696 | tf_op jit(solution)/shard_map/ppermute | solution.py:91
  183.9 47.2 %collective-permute-start.11 = (bf16[1408,256]{1,0:T(8,128)(2,1)}, bf16[1408,256]{1,0:T(8,128)(2,1)S(1)}, u32[]{:S(2)}, u32[]{:S(2)}) collective-permute-start(bf16[1408,256]{1,0:T(8,128)(2,1)} %copy-done.24), channel_id=1, source_target_pairs={{8,0},{16,8},{24,16},{28,24},{20,28},{12,20},{4,12},{0,4},{9,1},{1... | collective-permute-start | bytes 2162696 | tf_op jit(solution)/shard_map/ppermute | solution.py:91
  192.4 38.7 %copy-start.33 = (s32[8]{0:T(128)S(1)}, s32[8]{0:T(128)}, u32[]{:S(2)}) copy-start(s32[8]{0:T(128)} %constant.143.clone) | copy-start | bytes 100
  192.4 43.2 %copy-start.28 = (s32[8]{0:T(128)S(1)}, s32[8]{0:T(128)}, u32[]{:S(2)}) copy-start(s32[8]{0:T(128)} %constant.144.clone) | copy-start | bytes 100
  241.7 19.5 %collective-permute-start.12 = (bf16[128,2816]{1,0:T(8,128)(2,1)}, bf16[128,2816]{1,0:T(8,128)(2,1)S(1)}, u32[]{:S(2)}, u32[]{:S(2)}) collective-permute-start(bf16[128,2816]{1,0:T(8,128)(2,1)} %slice.78), channel_id=1, source_target_pairs={{0,8},{8,16},{16,24},{24,28},{28,20},{20,12},{12,4},{4,0},{1,9},{9... | collective-permute-start | bytes 2162696 | tf_op jit(solution)/shard_map/ppermute | solution.py:97
  244.1 19.3 %collective-permute-start.13 = (bf16[128,2816]{1,0:T(8,128)(2,1)}, bf16[128,2816]{1,0:T(8,128)(2,1)}, u32[]{:S(2)}, u32[]{:S(2)}) collective-permute-start(bf16[128,2816]{1,0:T(8,128)(2,1)} %slice.79), channel_id=1, source_target_pairs={{8,0},{16,8},{24,16},{28,24},{20,28},{12,20},{4,12},{0,4},{9,1},{1... | collective-permute-start | bytes 2162696 | tf_op jit(solution)/shard_map/ppermute | solution.py:98
  246.8 31.0 %collective-permute-start.14 = (bf16[704,256]{1,0:T(8,128)(2,1)S(1)}, bf16[704,256]{1,0:T(8,128)(2,1)}, u32[]{:S(2)}, u32[]{:S(2)}) collective-permute-start(bf16[704,256]{1,0:T(8,128)(2,1)S(1)} %slice.86), channel_id=1, source_target_pairs={{0,8},{8,16},{16,24},{24,28},{28,20},{20,12},{12,4},{4,0},{1,9},{9... | collective-permute-start | bytes 1081352 | tf_op jit(solution)/shard_map/ppermute | solution.py:97
  248.0 29.8 %collective-permute-start.15 = (bf16[704,256]{1,0:T(8,128)(2,1)}, bf16[704,256]{1,0:T(8,128)(2,1)}, u32[]{:S(2)}, u32[]{:S(2)}) collective-permute-start(bf16[704,256]{1,0:T(8,128)(2,1)} %slice.87), channel_id=1, source_target_pairs={{8,0},{16,8},{24,16},{28,24},{20,28},{12,20},{4,12},{0,4},{9,1},{1... | collective-permute-start | bytes 1081352 | tf_op jit(solution)/shard_map/ppermute | solution.py:98
  272.5 15.1 %all-to-all-start.1 = ((bf16[4,96,1024]{2,1,0:T(8,128)(2,1)}), bf16[4,96,1024]{2,1,0:T(8,128)(2,1)S(1)}, u32[]{:S(2)}, u32[]{:S(2)}) async-start(bf16[4,96,1024]{2,1,0:T(8,128)(2,1)} %bitcast.24), calls=%async_computation.1 | async-start | bytes 1572864 | tf_op jit(solution)/shard_map/all_to_all | solution.py:251
  287.6 15.1 %all-to-all-start.2 = ((bf16[4,96,1024]{2,1,0:T(8,128)(2,1)}), bf16[4,96,1024]{2,1,0:T(8,128)(2,1)S(1)}, u32[]{:S(2)}, u32[]{:S(2)}) async-start(bf16[4,96,1024]{2,1,0:T(8,128)(2,1)} %bitcast.25), calls=%async_computation.2 | async-start | bytes 1572864 | tf_op jit(solution)/shard_map/all_to_all | solution.py:251
  291.3 11.6 %copy-start.3 = (bf16[96,2048]{1,0:T(8,128)(2,1)S(1)}, bf16[96,2048]{1,0:T(8,128)(2,1)}, u32[]{:S(2)}) copy-start(bf16[96,2048]{1,0:T(8,128)(2,1)} %multiply_convert_fusion.1) | copy-start | bytes 1179652
  (23 other events, 52.6 us)
Sparse Core Ops, SparseCore 0:
  11.4 80.4 all-gather.2
  231.2 17.5 all-gather.4

commit v2 on v1

--- a/solution.py
+++ b/solution.py
@@ -136,8 +136,9 @@
     tp_count = lax.axis_size("tp")
     part_rows = tok_rows // tp_count
     tp_index = lax.axis_index("tp")
-    ring = Ring([jnp.concatenate([w_gate, w_up], axis=1), w_down])
-    ring.hop()
+    gate_ring = Ring([jnp.concatenate([w_gate, w_up], axis=1)])
+    down_ring = Ring([w_down])
+    gate_ring.hop()
     positions = lax.axis_index("sp") * tok_rows + jnp.arange(tok_rows, dtype=jnp.int32)
     cos_table, sin_table = rope_angles(positions)
     q_normed = rms_scaled(q_latent, q_gain)
@@ -195,13 +196,14 @@
         return attend_rows(carried, (key_piece, value_piece, rot_piece, doc_piece), between)
 
     def next_hop(value):
-        (value,) = ring.land(value)
-        ring.hop()
+        (value,) = gate_ring.land(value)
+        gate_ring.hop()
         return value
 
     doc_lanes = jnp.broadcast_to(doc_ids.astype(jnp.bfloat16)[:, None], (tok_rows, RD))
     packed = jnp.concatenate([kv_normed, key_rot, doc_lanes], axis=1)
-    packed_all = lax.all_gather(packed, "sp", axis=0, tiled=True)
+    packed_part = lax.dynamic_slice_in_dim(packed, tp_index * part_rows, part_rows, 0)
+    packed_all = lax.all_gather(packed_part, ("sp", "tp"), axis=0, tiled=True)
     packed_all = next_hop(packed_all)
     kv_rank = kv_latent.shape[1]
     gathered = (
@@ -225,29 +227,38 @@
     own_normed = layer_scaled(
         resid_alpha * own_resid.astype(jnp.float32) + mixer_out, mix_gain
     ).astype(jnp.bfloat16)
-    own_normed = next_hop(own_normed)
+    (own_normed,) = gate_ring.land(own_normed)
+    down_ring.hop()
+    gate_ring.hop()
     normed_rows = lax.all_gather(own_normed, "tp", axis=0, tiled=True)
-    ring.land()
-    while ring.step < ring.count // 2:
-        ring.hop()
-        ring.land()
-    gate_up, down = ring.pieces
+    (normed_rows,) = down_ring.land(normed_rows)
+    down_ring.hop()
+    gate_ring.land()
+    while gate_ring.step < gate_ring.count // 2:
+        gate_ring.hop()
+        gate_ring.land()
     gate_sum = None
-    for owner, piece in gate_up:
+    for owner, piece in gate_ring.pieces[0]:
         rows = lax.dynamic_slice_in_dim(normed_rows, owner * piece.shape[0], piece.shape[0], 1)
         term = jnp.dot(rows, piece, preferred_element_type=jnp.float32)
         gate_sum = term if gate_sum is None else gate_sum + term
     width = w_gate.shape[1]
     hidden = (jax.nn.silu(gate_sum[:, :width]) * gate_sum[:, width:]).astype(jnp.bfloat16)
+    (hidden,) = down_ring.land(hidden)
+    while down_ring.step < down_ring.count // 2:
+        down_ring.hop()
+        down_ring.land()
+    down = down_ring.pieces[0]
     ffn_sum = jnp.zeros((part_rows, resid_stream.shape[1]), jnp.float32)
-    for group in (down[: len(down) // 2], down[len(down) // 2 :]):
-        partial = jnp.concatenate(
-            [
-                jnp.dot(hidden, piece, preferred_element_type=jnp.float32).astype(jnp.bfloat16)
-                for _, piece in group
-            ],
-            axis=1,
-        )
+    for part, group in enumerate((down[: len(down) // 2], down[len(down) // 2 :])):
+        pieces = [piece for _, piece in group]
+        if part == 0:
+            pieces = [jnp.concatenate(pieces, axis=1)]
+        terms = [
+            jnp.dot(hidden, piece, preferred_element_type=jnp.float32).astype(jnp.bfloat16)
+            for piece in pieces
+        ]
+        partial = jnp.concatenate(terms, axis=1)
         swapped = lax.all_to_all(
             partial.reshape(tp_count, part_rows, -1), "tp", split_axis=0, concat_axis=0, tiled=True
         )

time: 312 us -> 293 us (0.939)
  waiting for transfers between devices: 165 us -> 152 us
    ppermute x6, waiting for transfers between devices: 137 us -> 97.1 us  [send(): lax.ppermute(one, 'sp', self.right)]
    all_gather x1, waiting for transfers between devices: 0.01 us -> 19.4 us  [body(): packed_all = lax.all_gather(packed_part, ('sp', 'tp'), axis=0, tiled=True)]
    ppermute x2, waiting for transfers between devices: 0.01 us -> 5.49 us  [send(): lax.ppermute(one[:one.shape[0] // 2], 'sp', self.right)]
    unnamed x70 -> x53, local copies, waits for them, and re-layouts: 7.44 us -> 2.88 us
    optimization_barrier x0 -> x1, local copies, waits for them, and re-layouts: none -> 4.41 us  [land(): values, self.flying = lax.optimization_barrier((values, self.flying))]
    reduce_sum x1, other arithmetic: 12.9 us -> 9.1 us  [attend_rows(): denom_sum = denom_sum * factor + jnp.sum(weights, axis=-1)]
    dot_general x1, matrix products: 6.61 us -> 2.93 us  [attend_rows(): jnp.einsum('hqk,khd->qhd', weights, values_heads, preferred_element_type=...]
    ppermute x6, starting transfers between devices: 1.23 us -> 4.43 us  [send(): lax.ppermute(two, 'sp', self.left)]
  transfers between devices with their start and end apart: 21 -> 21, of which waited for: 10 -> 19; matrix products, arithmetic and copies ran while one was open for 16% -> 14% of each run, Pallas kernels for 0% -> 0%
where the time goes in v2:
time: 293 us; the launch traced here: 292 us
  waiting for transfers between devices  152 us (52%)
  matrix products  54.6 us (19%)
  starting transfers between devices  28.3 us (10%)
  between operations  22.4 us (8%)
  other arithmetic  19.2 us (7%)
  local copies, waits for them, and re-layouts  15.5 us (5%)
    ppermute x6, waiting for transfers between devices, send(): lax.ppermute(one, 'sp', self.right)  97.1 us
    all_gather x1, waiting for transfers between devices, body(): packed_all = lax.all_gather(packed_part, ('sp', 'tp'), axis=0, tiled=True)  19.4 us
    all_to_all x2, waiting for transfers between devices, body(): lax.all_to_all(partial.reshape(tp_count, part_rows, -1), 'tp', split_axis...  18.6 us
    dot_general x1, matrix products, attend_rows(): jnp.einsum('qhd,khd->hqk', query_nope, keys_heads, preferred_element_type...  12.9 us
    dot_general x8, matrix products, body(): term = jnp.dot(rows, piece, preferred_element_type=jnp.float32)  12.4 us
    dot_general x5, matrix products, body(): jnp.dot(hidden, piece, preferred_element_type=jnp.float32)  9.75 us
    reduce_sum x1, other arithmetic, attend_rows(): denom_sum = denom_sum * factor + jnp.sum(weights, axis=-1)  9.1 us
    ppermute x6, starting transfers between devices, send(): lax.ppermute(one, 'sp', self.right)  9.07 us
  transfers between devices with their start and end apart: 21, of which 19 were waited for; matrix products, arithmetic and copies ran while one was open for 14% of the time, Pallas kernels for 0%

profile of v2, /device:TPU:0, one launch (start us, length us, event | category | flops | bytes accessed | tf_op | source)
XLA Modules:
  0.0 292.5 jit_solution(2804934297813108978)
XLA Ops:
  12.0 3.1 %collective-permute-start = (bf16[256,2816]{1,0:T(8,128)(2,1)S(1)}, bf16[256,2816]{1,0:T(8,128)(2,1)S(1)}, u32[]{:S(2)}, u32[]{:S(2)}) collective-permute-start(bf16[256,2816]{1,0:T(8,128)(2,1)S(1)} %constant_dynamic-update-slice_fusion), channel_id=1, source_target_pairs={{0,8},{8,16},{16,24},{24,28},{28,20},{20,12},{12,4},{4,0},{1,9},{9... | collective-permute-start | bytes 4325384 | tf_op jit(solution)/shard_map/ppermute | solution.py:91
  17.1 33.6 %collective-permute-done = bf16[256,2816]{1,0:T(8,128)(2,1)S(1)} collective-permute-done((bf16[256,2816]{1,0:T(8,128)(2,1)S(1)}, bf16[256,2816]{1,0:T(8,128)(2,1)S(1)}, u32[]{:S(2)}, u32[]{:S(2)}) %collective-permute-start) | collective-permute-done | bytes 1441824 | tf_op jit(solution)/shard_map/ppermute | solution.py:91
  53.0 19.4 %all-gather.3.cloned.1.call-done = bf16[3072,384]{1,0:T(8,128)(2,1)} async-done(((bf16[96,384]{1,0:T(8,128)(2,1)}), bf16[3072,384]{1,0:T(8,128)(2,1)}) %all-gather.3.cloned.1.call-update) | async-done | bytes 2359312 | tf_op jit(solution)/shard_map/all_gather | solution.py:206
  72.4 4.4 %copy.62 = bf16[3072,384]{0,1:T(8,128)(2,1)} copy(bf16[3072,384]{1,0:T(8,128)(2,1)} %all-gather.3.cloned.1.call-done) | data formatting | bytes 4718592 | tf_op jit(solution)/shard_map/optimization_barrier | solution.py:106
  79.3 8.9 %fusion.41 = f32[3072,384,4]{0,1,2:T(8,128)} fusion(bf16[3072,384]{0,1:T(8,128)(2,1)} %copy.62, bf16[384,4,32]{0,2,1:T(8,128)(2,1)S(1)} %get-tuple-element.38, bf16[384,4,32]{0,2,1:T(8,128)(2,1)S(1)} %get-tuple-element.37), kind=kOutput, calls=%fused_computation.66 | convolution fusion | flops 604372992 | bytes 19464192 | tf_op jit(solution)/shard_map/qhd,kd->hqk/dot_general | solution.py:167
  88.2 12.9 %fusion.77 = (f32[4,384]{1,0:T(4,128)S(1)}, f32[4,384,3072]{2,1,0:T(8,128)}) fusion(f32[3072,384,4]{0,1,2:T(8,128)} %fusion.41, bf16[3072,4,128]{0,2,1:T(8,128)(2,1)S(1)} %bitcast.68, f32[384,4,192]{0,2,1:T(8,128)} %bitcast.71, pred[384,3072]{1,0:T(8,128)(4,1)S(1)} %broadcast_compare_fusion), kind=kOutput, calls=%fused_computation.133 | convolution fusion | flops 1226832384 | bytes 42473472 | tf_op jit(solution)/shard_map/qhd,khd->hqk/dot_general | solution.py:162
  103.1 9.1 %fusion.2 = (f32[4,384]{1,0:T(4,128)S(1)}, bf16[4,384,3072]{2,1,0:T(8,128)(2,1)S(1)}) fusion(f32[4,384,3072]{2,1,0:T(8,128)} %get-tuple-element.55, f32[4,384]{1,0:T(4,128)S(1)} %get-tuple-element.42, pred[384,3072]{1,0:T(8,128)(4,1)S(1)} %broadcast_compare_fusion), kind=kLoop, calls=%fused_computation.4 | loop fusion | flops 18872832 | bytes 29503488 | tf_op jit(solution)/shard_map/reduce_sum | solution.py:174
  113.3 21.7 %collective-permute-done.2 = bf16[256,2816]{1,0:T(8,128)(2,1)S(1)} collective-permute-done((bf16[256,2816]{1,0:T(8,128)(2,1)}, bf16[256,2816]{1,0:T(8,128)(2,1)S(1)}, u32[]{:S(2)}, u32[]{:S(2)}) %collective-permute-start.2) | collective-permute-done | bytes 1441824 | tf_op jit(solution)/shard_map/ppermute | solution.py:91
  136.1 2.9 %fusion.29 = bf16[384,4,128]{0,2,1:T(8,128)(2,1)S(1)} fusion(bf16[3072,4,128]{0,2,1:T(8,128)(2,1)S(1)} %bitcast.69, bf16[4,384,3072]{2,1,0:T(8,128)(2,1)S(1)} %get-tuple-element.23, f32[384,4]{0,1:T(4,128)S(1)} %bitcast_add_fusion.1, f32[384,4]{0,1:T(4,128)S(1)} %get-tuple-element.41), kind=kOutput, calls=%fused_computation.39 | convolution fusion | flops 1208549376 | bytes 12988416 | tf_op jit(solution)/shard_map/hqk,khd->qhd/dot_general | solution.py:176
  140.2 3.5 %all-to-all-start = ((bf16[4,96,512]{2,1,0:T(8,128)(2,1)}), bf16[4,96,512]{2,1,0:T(8,128)(2,1)S(1)}, u32[]{:S(2)}, u32[]{:S(2)}) async-start(bf16[4,96,512]{2,1,0:T(8,128)(2,1)} %all_to_all.20), calls=%async_computation | async-start | bytes 786432 | tf_op jit(solution)/shard_map/all_to_all | solution.py:224
  145.8 5.2 %all-to-all-done = bf16[4,96,512]{2,1,0:T(8,128)(2,1)S(1)} async-done(((bf16[4,96,512]{2,1,0:T(8,128)(2,1)}), bf16[4,96,512]{2,1,0:T(8,128)(2,1)S(1)}, u32[]{:S(2)}, u32[]{:S(2)}) %all-to-all-start) | async-done | bytes 393248 | tf_op jit(solution)/shard_map/all_to_all | solution.py:224
  151.1 5.0 %fusion.78 = (f32[96]{0:T(128)S(1)}, f32[96,2048]{1,0:T(8,128)S(1)}) fusion(bf16[96,2048]{1,0:T(8,128)(2,1)S(1)} %bitcast.72, bf16[2048,2048]{1,0:T(8,128)(2,1)} %param.30, bf16[384,2048]{1,0:T(8,128)(2,1)} %param.20, s32[]{:T(128)S(6)} %select_n.162), kind=kOutput, calls=%fused_computation.134 | convolution fusion | flops 806092672 | bytes 9961860 | tf_op jit(solution)/shard_map/dot_general | solution.py:225
  157.3 20.5 %collective-permute-done.4 = bf16[256,2816]{1,0:T(8,128)(2,1)S(1)} collective-permute-done((bf16[256,2816]{1,0:T(8,128)(2,1)}, bf16[256,2816]{1,0:T(8,128)(2,1)S(1)}, u32[]{:S(2)}, u32[]{:S(2)}) %collective-permute-start.4) | collective-permute-done | bytes 1441824 | tf_op jit(solution)/shard_map/ppermute | solution.py:91
  192.4 2.0 slice.79
  195.2 2.6 collective-permute-done.6
  198.4 2.3 fusion.48
  200.8 2.2 fusion.57
  203.7 2.1 fusion.52
  209.4 2.7 fusion.6
  215.2 11.8 %collective-permute-done.10 = bf16[1408,256]{1,0:T(8,128)(2,1)} collective-permute-done((bf16[1408,256]{1,0:T(8,128)(2,1)}, bf16[1408,256]{1,0:T(8,128)(2,1)}, u32[]{:S(2)}, u32[]{:S(2)}) %collective-permute-start.10) | collective-permute-done | bytes 720928 | tf_op jit(solution)/shard_map/ppermute | solution.py:91
  227.9 4.3 %fusion.22 = bf16[384,1024]{1,0:T(8,128)(2,1)} fusion(bf16[384,1408]{1,0:T(8,128)(2,1)S(1)} %fusion.15, bf16[1408,256]{1,0:T(8,128)(2,1)} %collective-permute-done.10, bf16[1408,256]{1,0:T(8,128)(2,1)} %collective-permute-done.7, bf16[1408,256]{1,0:T(8,128)(2,1)} %collective-permute-done.6, bf16[1408,256]{1,0:T(8,128)(2,1)} %param.34), kind=kOutput, calls=%fused_computation.33 | convolution fusion | flops 1119223808 | bytes 4751360 | tf_op jit(solution)/shard_map/dot_general | solution.py:258
  232.2 3.5 %all-to-all-start.1 = ((bf16[4,96,1024]{2,1,0:T(8,128)(2,1)}), bf16[4,96,1024]{2,1,0:T(8,128)(2,1)S(1)}, u32[]{:S(2)}, u32[]{:S(2)}) async-start(bf16[4,96,1024]{2,1,0:T(8,128)(2,1)} %bitcast.23), calls=%async_computation.1 | async-start | bytes 1572864 | tf_op jit(solution)/shard_map/all_to_all | solution.py:262
  235.7 1.5 collective-permute-start.12
  237.8 2.4 convolution_convert_fusion.5
  240.2 7.1 %all-to-all-done.1 = bf16[4,96,1024]{2,1,0:T(8,128)(2,1)S(1)} async-done(((bf16[4,96,1024]{2,1,0:T(8,128)(2,1)}), bf16[4,96,1024]{2,1,0:T(8,128)(2,1)S(1)}, u32[]{:S(2)}, u32[]{:S(2)}) %all-to-all-start.1) | async-done | bytes 786464 | tf_op jit(solution)/shard_map/all_to_all | solution.py:262
  247.5 6.9 %collective-permute-done.12 = bf16[1408,256]{1,0:T(8,128)(2,1)S(1)} collective-permute-done((bf16[1408,256]{1,0:T(8,128)(2,1)}, bf16[1408,256]{1,0:T(8,128)(2,1)S(1)}, u32[]{:S(2)}, u32[]{:S(2)}) %collective-permute-start.12) | collective-permute-done | bytes 720928 | tf_op jit(solution)/shard_map/ppermute | solution.py:91
  254.4 1.5 collective-permute-start.14
  258.2 1.8 convolution_convert_fusion.3
  260.0 4.5 %collective-permute-done.14 = bf16[704,256]{1,0:T(8,128)(2,1)S(1)} collective-permute-done((bf16[704,256]{1,0:T(8,128)(2,1)S(1)}, bf16[704,256]{1,0:T(8,128)(2,1)S(1)}, u32[]{:S(2)}, u32[]{:S(2)}) %collective-permute-start.14) | collective-permute-done | bytes 360480 | tf_op jit(solution)/shard_map/ppermute | solution.py:97
  264.5 2.3 collective-permute-done.15
  268.7 3.6 %all-to-all-start.2 = ((bf16[4,96,1024]{2,1,0:T(8,128)(2,1)}), bf16[4,96,1024]{2,1,0:T(8,128)(2,1)S(1)}, u32[]{:S(2)}, u32[]{:S(2)}) async-start(bf16[4,96,1024]{2,1,0:T(8,128)(2,1)} %bitcast.24), calls=%async_computation.2 | async-start | bytes 1572864 | tf_op jit(solution)/shard_map/all_to_all | solution.py:262
  272.4 11.5 %all-to-all-done.2 = bf16[4,96,1024]{2,1,0:T(8,128)(2,1)S(1)} async-done(((bf16[4,96,1024]{2,1,0:T(8,128)(2,1)}), bf16[4,96,1024]{2,1,0:T(8,128)(2,1)S(1)}, u32[]{:S(2)}, u32[]{:S(2)}) %all-to-all-start.2) | async-done | bytes 786464 | tf_op jit(solution)/shard_map/all_to_all | solution.py:262
  (139 shorter events, 43.0 us)
Async XLA Ops:
  6.5 8.7 %copy-start = (bf16[512,768]{1,0:T(8,128)(2,1)S(1)}, bf16[512,768]{1,0:T(8,128)(2,1)}, u32[]{:S(2)}) copy-start(bf16[512,768]{1,0:T(8,128)(2,1)} %param.27) | copy-start | bytes 2359300
  6.5 65.9 %all-gather.3.cloned.1.call-start = ((), (), s32[]{:S(2)}) async-start(), calls=%async_computation.3 | async-start | bytes 2433024 | tf_op jit(solution)/shard_map/all_gather | solution.py:206
  7.9 7.2 %copy-start.7 = (bf16[384,512]{1,0:T(8,128)(2,1)S(1)}, bf16[384,512]{1,0:T(8,128)(2,1)}, u32[]{:S(2)}) copy-start(bf16[384,512]{1,0:T(8,128)(2,1)} %param.21) | copy-start | bytes 1179652
  9.9 5.4 %copy-start.24 = (f32[512]{0:T(512)S(1)}, f32[512]{0:T(512)}, u32[]{:S(2)}) copy-start(f32[512]{0:T(512)} %param.25) | copy-start | bytes 6148
  12.0 38.7 %collective-permute-start = (bf16[256,2816]{1,0:T(8,128)(2,1)S(1)}, bf16[256,2816]{1,0:T(8,128)(2,1)S(1)}, u32[]{:S(2)}, u32[]{:S(2)}) collective-permute-start(bf16[256,2816]{1,0:T(8,128)(2,1)S(1)} %constant_dynamic-update-slice_fusion), channel_id=1, source_target_pairs={{0,8},{8,16},{16,24},{24,28},{28,20},{20,12},{12,4},{4,0},{1,9},{9... | collective-permute-start | bytes 4325384 | tf_op jit(solution)/shard_map/ppermute | solution.py:91
  15.1 37.9 %collective-permute-start.1 = (bf16[256,2816]{1,0:T(8,128)(2,1)S(1)}, bf16[256,2816]{1,0:T(8,128)(2,1)}, u32[]{:S(2)}, u32[]{:S(2)}) collective-permute-start(bf16[256,2816]{1,0:T(8,128)(2,1)S(1)} %constant_dynamic-update-slice_fusion), channel_id=1, source_target_pairs={{8,0},{16,8},{24,16},{28,24},{20,28},{12,20},{4,12},{0,4},{9,1},{1... | collective-permute-start | bytes 4325384 | tf_op jit(solution)/shard_map/ppermute | solution.py:91
  17.1 60.5 %copy-start.23 = (s32[384]{0:T(512)S(1)}, s32[384]{0:T(512)}, u32[]{:S(2)}) copy-start(s32[384]{0:T(512)} %param.24) | copy-start | bytes 4612
  101.1 34.0 %collective-permute-start.2 = (bf16[256,2816]{1,0:T(8,128)(2,1)}, bf16[256,2816]{1,0:T(8,128)(2,1)S(1)}, u32[]{:S(2)}, u32[]{:S(2)}) collective-permute-start(bf16[256,2816]{1,0:T(8,128)(2,1)} %copy-done.11), channel_id=1, source_target_pairs={{0,8},{8,16},{16,24},{24,28},{28,20},{20,12},{12,4},{4,0},{1,9},{9... | collective-permute-start | bytes 4325384 | tf_op jit(solution)/shard_map/ppermute | solution.py:91
  101.9 33.8 %collective-permute-start.3 = (bf16[256,2816]{1,0:T(8,128)(2,1)}, bf16[256,2816]{1,0:T(8,128)(2,1)}, u32[]{:S(2)}, u32[]{:S(2)}) collective-permute-start(bf16[256,2816]{1,0:T(8,128)(2,1)} %collective-permute-done.1), channel_id=1, source_target_pairs={{8,0},{16,8},{24,16},{28,24},{20,28},{12,20},{4,12},{0,4},{9,1},{1... | collective-permute-start | bytes 4325384 | tf_op jit(solution)/shard_map/ppermute | solution.py:91
  103.1 9.1 %copy-start.19 = (bf16[256,512]{1,0:T(8,128)(2,1)S(1)}, bf16[256,512]{1,0:T(8,128)(2,1)}, u32[]{:S(2)}) copy-start(bf16[256,512]{1,0:T(8,128)(2,1)} %param.29) | copy-start | bytes 786436
  140.2 10.8 %all-to-all-start = ((bf16[4,96,512]{2,1,0:T(8,128)(2,1)}), bf16[4,96,512]{2,1,0:T(8,128)(2,1)S(1)}, u32[]{:S(2)}, u32[]{:S(2)}) async-start(bf16[4,96,512]{2,1,0:T(8,128)(2,1)} %all_to_all.20), calls=%async_computation | async-start | bytes 786432 | tf_op jit(solution)/shard_map/all_to_all | solution.py:224
  143.7 54.7 %all-gather.5.cloned.1.call-start = ((), (), s32[]{:S(2)}) async-start(), calls=%async_computation.4 | async-start | bytes 1966080 | tf_op jit(solution)/shard_map/all_gather | solution.py:233
  143.7 34.1 %collective-permute-start.4 = (bf16[256,2816]{1,0:T(8,128)(2,1)}, bf16[256,2816]{1,0:T(8,128)(2,1)S(1)}, u32[]{:S(2)}, u32[]{:S(2)}) collective-permute-start(bf16[256,2816]{1,0:T(8,128)(2,1)} %copy-done.12), channel_id=1, source_target_pairs={{0,8},{8,16},{16,24},{24,28},{28,20},{20,12},{12,4},{4,0},{1,9},{9... | collective-permute-start | bytes 4325384 | tf_op jit(solution)/shard_map/ppermute | solution.py:91
  144.6 33.9 %collective-permute-start.5 = (bf16[256,2816]{1,0:T(8,128)(2,1)}, bf16[256,2816]{1,0:T(8,128)(2,1)}, u32[]{:S(2)}, u32[]{:S(2)}) collective-permute-start(bf16[256,2816]{1,0:T(8,128)(2,1)} %collective-permute-done.3), channel_id=1, source_target_pairs={{8,0},{16,8},{24,16},{28,24},{20,28},{12,20},{4,12},{0,4},{9,1},{1... | collective-permute-start | bytes 4325384 | tf_op jit(solution)/shard_map/ppermute | solution.py:91
  156.1 24.4 %copy-start.25 = (s32[8]{0:T(128)S(1)}, s32[8]{0:T(128)}, u32[]{:S(2)}) copy-start(s32[8]{0:T(128)} %constant.171.clone) | copy-start | bytes 100
  156.1 29.0 %copy-start.20 = (s32[8]{0:T(128)S(1)}, s32[8]{0:T(128)}, u32[]{:S(2)}) copy-start(s32[8]{0:T(128)} %constant.172.clone) | copy-start | bytes 100
  178.5 19.4 %collective-permute-start.6 = (bf16[1408,256]{1,0:T(8,128)(2,1)}, bf16[1408,256]{1,0:T(8,128)(2,1)}, u32[]{:S(2)}, u32[]{:S(2)}) collective-permute-start(bf16[1408,256]{1,0:T(8,128)(2,1)} %param.34), channel_id=1, source_target_pairs={{0,8},{8,16},{16,24},{24,28},{28,20},{20,12},{12,4},{4,0},{1,9},{9... | collective-permute-start | bytes 2162696 | tf_op jit(solution)/shard_map/ppermute | solution.py:91
  179.8 18.7 %collective-permute-start.7 = (bf16[1408,256]{1,0:T(8,128)(2,1)}, bf16[1408,256]{1,0:T(8,128)(2,1)}, u32[]{:S(2)}, u32[]{:S(2)}) collective-permute-start(bf16[1408,256]{1,0:T(8,128)(2,1)} %param.34), channel_id=1, source_target_pairs={{8,0},{16,8},{24,16},{28,24},{20,28},{12,20},{4,12},{0,4},{9,1},{1... | collective-permute-start | bytes 2162696 | tf_op jit(solution)/shard_map/ppermute | solution.py:91
  191.2 22.0 %collective-permute-start.8 = (bf16[128,2816]{1,0:T(8,128)(2,1)}, bf16[128,2816]{1,0:T(8,128)(2,1)S(1)}, u32[]{:S(2)}, u32[]{:S(2)}) collective-permute-start(bf16[128,2816]{1,0:T(8,128)(2,1)} %slice.78), channel_id=1, source_target_pairs={{0,8},{8,16},{16,24},{24,28},{28,20},{20,12},{12,4},{4,0},{1,9},{9... | collective-permute-start | bytes 2162696 | tf_op jit(solution)/shard_map/ppermute | solution.py:97
  194.4 19.3 %collective-permute-start.9 = (bf16[128,2816]{1,0:T(8,128)(2,1)}, bf16[128,2816]{1,0:T(8,128)(2,1)S(1)}, u32[]{:S(2)}, u32[]{:S(2)}) collective-permute-start(bf16[128,2816]{1,0:T(8,128)(2,1)} %slice.79), channel_id=1, source_target_pairs={{8,0},{16,8},{24,16},{28,24},{20,28},{12,20},{4,12},{0,4},{9,1},{1... | collective-permute-start | bytes 2162696 | tf_op jit(solution)/shard_map/ppermute | solution.py:98
  206.6 20.4 %collective-permute-start.10 = (bf16[1408,256]{1,0:T(8,128)(2,1)}, bf16[1408,256]{1,0:T(8,128)(2,1)}, u32[]{:S(2)}, u32[]{:S(2)}) collective-permute-start(bf16[1408,256]{1,0:T(8,128)(2,1)} %collective-permute-done.6), channel_id=1, source_target_pairs={{0,8},{8,16},{16,24},{24,28},{28,20},{20,12},{12,4},{4,0},{1,9},{9... | collective-permute-start | bytes 2162696 | tf_op jit(solution)/shard_map/ppermute | solution.py:91
  208.1 19.7 %collective-permute-start.11 = (bf16[1408,256]{1,0:T(8,128)(2,1)}, bf16[1408,256]{1,0:T(8,128)(2,1)S(1)}, u32[]{:S(2)}, u32[]{:S(2)}) collective-permute-start(bf16[1408,256]{1,0:T(8,128)(2,1)} %collective-permute-done.7), channel_id=1, source_target_pairs={{8,0},{16,8},{24,16},{28,24},{20,28},{12,20},{4,12},{0,4},{9,1},{1... | collective-permute-start | bytes 2162696 | tf_op jit(solution)/shard_map/ppermute | solution.py:91
  232.2 15.1 %all-to-all-start.1 = ((bf16[4,96,1024]{2,1,0:T(8,128)(2,1)}), bf16[4,96,1024]{2,1,0:T(8,128)(2,1)S(1)}, u32[]{:S(2)}, u32[]{:S(2)}) async-start(bf16[4,96,1024]{2,1,0:T(8,128)(2,1)} %bitcast.23), calls=%async_computation.1 | async-start | bytes 1572864 | tf_op jit(solution)/shard_map/all_to_all | solution.py:262
  235.7 18.7 %collective-permute-start.12 = (bf16[1408,256]{1,0:T(8,128)(2,1)}, bf16[1408,256]{1,0:T(8,128)(2,1)S(1)}, u32[]{:S(2)}, u32[]{:S(2)}) collective-permute-start(bf16[1408,256]{1,0:T(8,128)(2,1)} %collective-permute-done.10), channel_id=1, source_target_pairs={{0,8},{8,16},{16,24},{24,28},{28,20},{20,12},{12,4},{4,0},{1,9},{9... | collective-permute-start | bytes 2162696 | tf_op jit(solution)/shard_map/ppermute | solution.py:91
  237.2 18.8 %collective-permute-start.13 = (bf16[1408,256]{1,0:T(8,128)(2,1)}, bf16[1408,256]{1,0:T(8,128)(2,1)}, u32[]{:S(2)}, u32[]{:S(2)}) collective-permute-start(bf16[1408,256]{1,0:T(8,128)(2,1)} %copy-done.17), channel_id=1, source_target_pairs={{8,0},{16,8},{24,16},{28,24},{20,28},{12,20},{4,12},{0,4},{9,1},{1... | collective-permute-start | bytes 2162696 | tf_op jit(solution)/shard_map/ppermute | solution.py:91
  247.4 7.0 %copy-start.8 = (f32[96,1024]{1,0:T(8,128)}, f32[96,1024]{1,0:T(8,128)S(1)}, u32[]{:S(2)}) copy-start(f32[96,1024]{1,0:T(8,128)S(1)} %convert_reduce_fusion.2) | copy-start | bytes 1179652
  254.4 10.0 %collective-permute-start.14 = (bf16[704,256]{1,0:T(8,128)(2,1)S(1)}, bf16[704,256]{1,0:T(8,128)(2,1)S(1)}, u32[]{:S(2)}, u32[]{:S(2)}) collective-permute-start(bf16[704,256]{1,0:T(8,128)(2,1)S(1)} %slice.104), channel_id=1, source_target_pairs={{0,8},{8,16},{16,24},{24,28},{28,20},{20,12},{12,4},{4,0},{1,9},{9... | collective-permute-start | bytes 1081352 | tf_op jit(solution)/shard_map/ppermute | solution.py:97
  257.0 9.8 %collective-permute-start.15 = (bf16[704,256]{1,0:T(8,128)(2,1)S(1)}, bf16[704,256]{1,0:T(8,128)(2,1)S(1)}, u32[]{:S(2)}, u32[]{:S(2)}) collective-permute-start(bf16[704,256]{1,0:T(8,128)(2,1)S(1)} %slice.105), channel_id=1, source_target_pairs={{8,0},{16,8},{24,16},{28,24},{20,28},{12,20},{4,12},{0,4},{9,1},{1... | collective-permute-start | bytes 1081352 | tf_op jit(solution)/shard_map/ppermute | solution.py:98
  258.2 9.2 %copy-start.14 = (bf16[384,256]{0,1:T(8,128)(2,1)S(1)}, bf16[384,256]{0,1:T(8,128)(2,1)}, u32[]{:S(2)}) copy-start(bf16[384,256]{0,1:T(8,128)(2,1)} %convolution_convert_fusion.5) | copy-start | bytes 589828
  268.7 15.5 %copy-start.3 = (bf16[96,2048]{1,0:T(8,128)(2,1)S(1)}, bf16[96,2048]{1,0:T(8,128)(2,1)}, u32[]{:S(2)}) copy-start(bf16[96,2048]{1,0:T(8,128)(2,1)} %multiply_convert_fusion.1) | copy-start | bytes 1179652
  268.7 15.2 %all-to-all-start.2 = ((bf16[4,96,1024]{2,1,0:T(8,128)(2,1)}), bf16[4,96,1024]{2,1,0:T(8,128)(2,1)S(1)}, u32[]{:S(2)}, u32[]{:S(2)}) async-start(bf16[4,96,1024]{2,1,0:T(8,128)(2,1)} %bitcast.24), calls=%async_computation.2 | async-start | bytes 1572864 | tf_op jit(solution)/shard_map/all_to_all | solution.py:262
  272.4 12.3 %copy-start.22 = (f32[2048]{0:T(1024)S(1)}, f32[2048]{0:T(1024)}, u32[]{:S(2)}) copy-start(f32[2048]{0:T(1024)} %param.35) | copy-start | bytes 24580
  (15 other events, 48.3 us)
Sparse Core Ops, SparseCore 0:
  11.9 60.4 all-gather.2
  178.6 19.3 all-gather.4
